TPU v7x, 256 devices: a whole 4x4x8 slice. The times are simulated.
256 devices in a mesh: ep: 16 (over y, x), tp: 16 (over z, core).
Axes of the slice: x: 4, y: 4, z: 8, core: 2. Of those that a mesh axis runs over, the one named last changes fastest.
Arguments:
- queries: bfloat16 [12288, 2048], P('ep', 'tp'), may hold values from -6 to 6
- keys: bfloat16 [12288, 512], P('ep'), may hold values from -6 to 6
- values: bfloat16 [12288, 512], P('ep'), may hold values from -6 to 6
- query_gain: float32 [128], replicated, may hold values from 1 to 4.5
- key_gain: float32 [128], replicated, may hold values from 1 to 4.5
- out_weight: bfloat16 [2048, 2048], P('tp'), may hold values from -0.75 to 0.75
- tokens_b: bfloat16 [12288, 2048], P('ep'), may hold values from -6 to 6
- norm_gain: float32 [2048], replicated, may hold values from 0.1 to 1.9
- routes: int32 [12288, 2], P('ep'), may hold values from 0 to 15, all different within a row; in each aligned block of 48 rows (0 to 47, 48 to 95, ...) at most 8 rows name the same one
- route_weight: float32 [12288, 2], P('ep'), may hold values from 0.2 to 1
- gate_weight: bfloat16 [16, 2048, 4096], P('ep', None, 'tp'), may hold values from -0.125 to 0.125
- up_weight: bfloat16 [16, 2048, 4096], P('ep', None, 'tp'), may hold values from -0.125 to 0.125
- down_weight: bfloat16 [16, 4096, 2048], P('ep', 'tp'), may hold values from -0.09375 to 0.09375
Outputs:
- mixed_out: bfloat16 [12288, 2048], P(('ep', 'tp'))
- expert_out: bfloat16 [12288, 2048], P(('ep', 'tp'))
Inputs may be any that keep to these rules, and one draw needn't show every extreme that they name: `routes`: A row names 2 different experts. In each aligned block of 48 rows no expert is named more than 8 times, a bound that some block reaches.
All inputs are finite; a program needn't handle non-finite values.
Results may differ from a plain program's by a relative error of at most 0.019.
Values may be sent and summed in bfloat16 or wider, within the bound.
A program may use at most 128 MiB of HBM per device.

v0:
```python
import jax
import jax.numpy as jnp
from jax import lax
from jax.sharding import Mesh
from jax.sharding import PartitionSpec as P

D = 2048
HD = 128
HQ = 16
KVH = 4
EXPERTS = 16
TOPK = 2
GRID_W = 64
CAP = 8
TP = ("tp_0", "tp_1")
EP_TP = ("ep", "tp_0", "tp_1")
EPS = 1e-06
THETA = 10000.0


def side_by_side(arrays, axis, dim, along):
    ends, at = ([], 0)
    for a in arrays[:-1]:
        at += a.shape[along]
        ends.append(at)
    both = jnp.concatenate(arrays, axis=along)
    return tuple(jnp.split(lax.all_gather(both, axis, axis=dim, tiled=True), ends, axis=along))


def sum_in_order(blocks, axes, sequence):
    inside = blocks.shape[1:]
    blocks = blocks.reshape(*(lax.axis_size(a) for a in axes), *inside)
    blocks = jnp.moveaxis(blocks, sequence, range(len(axes))).reshape(-1, *inside)
    for k in sequence:
        blocks = lax.psum_scatter(blocks, axes[k], scatter_dimension=0, tiled=True)
    return blocks[0]


def split_up(x, dim, size):
    before, after = (x.shape[:dim], x.shape[dim + 1 :])
    return jnp.moveaxis(x.reshape(*before, size, -1, *after), dim, 0)


def scatter_axes(x, axes, sequence, dim):
    size = lax.axis_size(axes)
    return sum_in_order(split_up(x, dim, size), axes, sequence)


def rotate(field, positions):
    n_freq = HD // 4
    row_pos = (positions // GRID_W).astype(jnp.float32)
    col_pos = (positions % GRID_W).astype(jnp.float32)
    inverse = THETA ** (-jnp.arange(n_freq, dtype=jnp.float32) / n_freq)
    angles = jnp.stack([row_pos[:, None] * inverse, col_pos[:, None] * inverse], axis=1)
    cosine = jnp.cos(angles)[:, None]
    sine = jnp.sin(angles)[:, None]
    length, n_heads = (field.shape[0], field.shape[1])
    halves = field.reshape(length, n_heads, 2, 2, n_freq)
    leading = halves[..., 0, :]
    second = halves[..., 1, :]
    turned = jnp.stack(
        [leading * cosine - second * sine, second * cosine + leading * sine], axis=-2
    )
    return turned.reshape(length, n_heads, HD)


def prepare(source, gain_vec, positions, n_heads):
    length = source.shape[0]
    field = source.astype(jnp.float32).reshape(length, n_heads, HD)
    field = field * lax.rsqrt(jnp.mean(field * field, axis=-1, keepdims=True) + EPS) * gain_vec
    return rotate(field, positions).astype(jnp.bfloat16)


def token_mixer(queries, keys, values, query_gain, key_gain, out_weight):
    n_rows = queries.shape[0]
    q_heads = queries.shape[1] // HD
    positions = lax.axis_index("ep") * n_rows + jnp.arange(n_rows, dtype=jnp.int32)
    query_n = prepare(queries, query_gain, positions, q_heads).reshape(n_rows * q_heads, HD)
    kv_index = lax.axis_index(TP) * q_heads // (HQ // KVH)
    own_keys = prepare(
        lax.dynamic_slice_in_dim(keys, kv_index * HD, HD, 1), key_gain, positions, 1
    ).reshape(n_rows, HD)
    own_values = lax.dynamic_slice_in_dim(values, kv_index * HD, HD, 1)
    score_scale = HD ** (-0.5)
    start_state = (
        jnp.full((n_rows * q_heads,), -1e30, jnp.float32),
        jnp.zeros((n_rows * q_heads,), jnp.float32),
        jnp.zeros((n_rows * q_heads, HD), jnp.float32),
    )
    key_piece, value_piece = side_by_side((own_keys, own_values), "ep", 0, 1)
    steps_n = key_piece.shape[0] // n_rows

    def one_block(index_b, state):
        running_max, totals, numerator = state
        key_blk = lax.dynamic_slice_in_dim(key_piece, index_b * n_rows, n_rows, 0)
        value_blk = lax.dynamic_slice_in_dim(value_piece, index_b * n_rows, n_rows, 0)
        scores = (
            jnp.einsum("qd,sd->qs", query_n, key_blk, preferred_element_type=jnp.float32)
            * score_scale
        )
        new_max = jnp.maximum(running_max, jnp.max(scores, axis=1))
        shrink = jnp.exp(running_max - new_max)
        weights = jnp.exp(scores - new_max[:, None])
        totals = totals * shrink + jnp.sum(weights, axis=1)
        numerator = numerator * shrink[:, None] + jnp.dot(
            weights.astype(jnp.bfloat16), value_blk, preferred_element_type=jnp.float32
        )
        return (new_max, totals, numerator)

    running_max, totals, numerator = lax.fori_loop(0, steps_n, one_block, start_state)
    attended = (numerator / totals[:, None]).astype(jnp.bfloat16)
    own_rows = lax.all_to_all(attended, TP, split_axis=0, concat_axis=1, tiled=True)
    return jnp.dot(
        own_rows,
        lax.all_gather(out_weight, TP, axis=0, tiled=True),
        preferred_element_type=jnp.float32,
    ).astype(jnp.bfloat16)


def expert_half(tokens_b, norm_gain, routes, route_weight, gate_weight, up_weight, down_weight):
    n_tp = lax.axis_size(TP)
    n_ep = lax.axis_size("ep")
    tp_index = lax.axis_index(TP)
    local_rows = tokens_b.shape[0]
    block_rows = local_rows // n_tp
    picks = block_rows * TOPK
    local_experts = gate_weight.shape[0]
    assigned = routes.reshape(n_tp, picks)
    onehot = (assigned[:, :, None] == jnp.arange(EXPERTS, dtype=jnp.int32)[None, None, :]).astype(
        jnp.int32
    )
    slot_rank = jnp.sum((jnp.cumsum(onehot, axis=1) - onehot) * onehot, axis=-1)
    target = assigned * CAP + slot_rank
    target_hot = (
        target[:, :, None] == jnp.arange(EXPERTS * CAP, dtype=jnp.int32)[None, None, :]
    ).astype(jnp.float32)
    token_hot = (
        jnp.arange(picks, dtype=jnp.int32)[:, None] // TOPK
        == jnp.arange(block_rows, dtype=jnp.int32)[None, :]
    ).astype(jnp.float32)
    own_block = lax.dynamic_slice_in_dim(tokens_b, tp_index * block_rows, block_rows, 0)
    field = own_block.astype(jnp.float32)
    own_normed = (
        field * lax.rsqrt(jnp.mean(field * field, axis=-1, keepdims=True) + EPS) * norm_gain
    ).astype(jnp.bfloat16)
    own_hot = lax.dynamic_index_in_dim(target_hot, tp_index, 0, keepdims=False)
    own_mat = jnp.einsum("aj,at->jt", own_hot, token_hot, precision=lax.Precision.HIGHEST).astype(
        jnp.bfloat16
    )
    outgoing = jnp.dot(own_mat, own_normed, preferred_element_type=jnp.float32)
    outgoing = outgoing.astype(jnp.bfloat16).reshape(EXPERTS, CAP, D)
    arrived = lax.all_to_all(outgoing, "ep", split_axis=0, concat_axis=1, tiled=True)
    arrived = arrived.reshape(1, local_experts, n_ep * CAP, D)
    slab_rows = lax.all_gather(arrived, TP, axis=0, tiled=True)
    gate_act = jnp.einsum(
        "blmd,ldf->blmf", slab_rows, gate_weight, preferred_element_type=jnp.float32
    )
    up_act = jnp.einsum("blmd,ldf->blmf", slab_rows, up_weight, preferred_element_type=jnp.float32)
    hidden = (jax.nn.silu(gate_act) * up_act).astype(jnp.bfloat16)
    result = jnp.einsum("blmf,lfd->blmd", hidden, down_weight, preferred_element_type=jnp.float32)
    terms = result.reshape(-1, D)
    summed = (
        scatter_axes(terms.astype(jnp.bfloat16), TP, (1, 0), 0)
        .astype(jnp.float32)
        .astype(jnp.bfloat16)
    )
    returned = lax.all_to_all(
        summed.reshape(local_experts, n_ep, CAP, D), "ep", split_axis=1, concat_axis=0, tiled=True
    )
    returned = returned.reshape(EXPERTS * CAP, D)
    own_target = lax.dynamic_index_in_dim(target_hot, tp_index, 0, keepdims=False)
    shares = (route_weight / jnp.sum(route_weight, axis=-1, keepdims=True)).reshape(n_tp, picks)
    own_shares = lax.dynamic_index_in_dim(shares, tp_index, 0, keepdims=False)
    combine = jnp.einsum(
        "at,aj->tj", token_hot, own_target * own_shares[:, None], precision=lax.Precision.HIGHEST
    )
    return jnp.dot(combine, returned.astype(jnp.float32), precision=lax.Precision.HIGHEST).astype(
        jnp.bfloat16
    )


def on_device(
    queries,
    keys,
    values,
    query_gain,
    key_gain,
    out_weight,
    tokens_b,
    norm_gain,
    routes,
    route_weight,
    gate_weight,
    up_weight,
    down_weight,
):
    mixed_out = token_mixer(queries, keys, values, query_gain, key_gain, out_weight)
    expert_out = expert_half(
        tokens_b, norm_gain, routes, route_weight, gate_weight, up_weight, down_weight
    )
    return (mixed_out, expert_out)


def solution(mesh):
    torus = Mesh(mesh.devices.reshape(mesh.shape["ep"], 8, 2), ("ep", "tp_0", "tp_1"))
    in_specs = (
        P("ep", TP),
        P("ep", None),
        P("ep", None),
        P(),
        P(),
        P(TP, None),
        P("ep", None),
        P(),
        P("ep", None),
        P("ep", None),
        P("ep", None, TP),
        P("ep", None, TP),
        P("ep", TP, None),
    )
    out_specs = (P(EP_TP, None), P(EP_TP, None))
    return jax.shard_map(
        on_device, mesh=torus, in_specs=in_specs, out_specs=out_specs, check_vma=False
    )
```

profile of v0, /device:TPU:1, one launch (start us, length us, event | category | flops | bytes accessed | tf_op | source)
XLA Modules:
  0.0 291.4 jit_solution(9098463858573012935)
XLA Ops:
  8.1 1.0 copy.49
  9.4 2.1 select_reduce_fusion
  11.9 1.1 fusion.42
  13.3 1.3 fusion.16
  14.6 17.9 %all_to_all.37 = bf16[16,8,2048]{2,1,0:T(8,128)(2,1)} all-to-all(bf16[16,8,2048]{2,1,0:T(8,128)(2,1)S(1)} %fusion.16), channel_id=1, replica_groups=mesh['ep'=16,'tp_0'=8,'tp_1'=2] {'ep'}, dimensions={0} | all-to-all | bytes 1048576 | tf_op jit(solution)/shard_map/all_to_all | solution.py:152
  32.6 56.8 %all-gather.8.cloned.1.call-done = bf16[16,1,128,2048]{3,2,1,0:T(8,128)(2,1)} async-done(((bf16[1,1,128,2048]{3,2,1,0:T(8,128)(2,1)}), bf16[16,1,128,2048]{3,2,1,0:T(8,128)(2,1)}) %all-gather.8.cloned.1.call-update) | async-done | bytes 8388624 | tf_op jit(solution)/shard_map/all_gather | solution.py:154
  89.4 7.1 %fusion.14 = f32[16,128,256]{2,1,0:T(8,128)} fusion(bf16[16,1,128,2048]{3,2,1,0:T(8,128)(2,1)} %all-gather.8.cloned.1.call-done, bf16[1,2048,256]{2,1,0:T(8,128)(2,1)S(1)} %copy-done.7), kind=kOutput, calls=%fused_computation.20 | convolution fusion | flops 2147483648 | bytes 11534336 | tf_op jit(solution)/shard_map/blmd,ldf->blmf/dot_general | solution.py:155
  96.5 13.2 %convolution_convert_fusion = bf16[16,128,2048]{2,1,0:T(8,128)(2,1)} fusion(bf16[16,1,128,2048]{3,2,1,0:T(8,128)(2,1)} %all-gather.8.cloned.1.call-done, f32[16,128,256]{2,1,0:T(8,128)} %fusion.14, bf16[1,256,2048]{2,1,0:T(8,128)(2,1)S(1)} %copy-done, bf16[1,2048,256]{2,1,0:T(8,128)(2,1)S(1)} %copy-done.8), kind=kOutput, calls=%fused_computation.22 | convolution fusion | flops 4302307328 | bytes 20971520 | tf_op jit(solution)/shard_map/blmf,lfd->blmd/dot_general | solution.py:160
  109.8 8.3 %copy.53 = bf16[8,2,128,2048]{3,2,0,1:T(8,128)(2,1)} copy(bf16[8,2,128,2048]{3,2,1,0:T(8,128)(2,1)} %bitcast.112) | data formatting | bytes 16777216 | tf_op jit(solution)/shard_map/convert_element_type | solution.py:163
  118.2 1.1 constant_dynamic-slice_fusion.1
  120.2 0.8 subtract_convert_fusion
  121.0 0.8 pad_maximum_fusion
  121.8 16.9 %reduce-scatter.3.cloned.1.call-done = bf16[8,128,2048]{2,1,0:T(8,128)(2,1)} async-done(((bf16[16,128,2048]{2,1,0:T(8,128)(2,1)}), bf16[8,128,2048]{2,1,0:T(8,128)(2,1)}) %reduce-scatter.3.cloned.1.call-update) | async-done | bytes 4194320 | tf_op jit(solution)/shard_map/reduce_scatter | solution.py:35
  139.6 46.2 %all-gather.4.cloned.1.call-done = bf16[12288,256]{0,1:T(8,128)(2,1)} async-done(((bf16[768,256]{0,1:T(8,128)(2,1)}), bf16[12288,256]{0,1:T(8,128)(2,1)}) %all-gather.4.cloned.1.call-update) | async-done | bytes 6291472 | tf_op jit(solution)/shard_map/all_gather | solution.py:27
  185.9 6.2 %fusion.74 = (bf16[12288,128]{0,1:T(8,128)(2,1)}, bf16[12288,128]{0,1:T(8,128)(2,1)}) fusion(bf16[12288,256]{0,1:T(8,128)(2,1)} %all-gather.4.cloned.1.call-done), kind=kLoop, calls=%fused_computation.121 | loop fusion | bytes 12582912 | tf_op jit(solution)/shard_map/split | solution.py:27
  192.1 55.9 %while.18 = (s32[]{:T(128)}, f32[768]{0:T(1024)S(1)}, f32[768]{0:T(1024)S(1)}, f32[768,128]{1,0:T(8,128)S(1)}, bf16[12288,128]{0,1:T(8,128)(2,1)}, /*index=5*/bf...) while((s32[]{:T(128)}, f32[768]{0:T(1024)S(1)}, ...), condition=%wide.region_5.6_spmd.clone, body=%wide.region_2.5_spmd.clone.sunk | while | flops 307007232 | bytes 8503471 | solution.py:110
  192.1 1.4 multiply_reduce_fusion.2
  193.6 0.4 fusion.88
  194.0 1.6 convolution_add_fusion.2
  195.6 1.4 multiply_reduce_fusion.2
  197.1 0.4 fusion.88
  197.5 1.6 convolution_add_fusion.2
  199.1 1.4 multiply_reduce_fusion.2
  201.0 1.6 convolution_add_fusion.2
  202.6 1.4 multiply_reduce_fusion.2
  204.0 0.4 fusion.88
  204.5 1.6 convolution_add_fusion.2
  206.1 1.4 multiply_reduce_fusion.2
  207.5 0.4 fusion.88
  208.0 1.6 convolution_add_fusion.2
  209.6 1.5 multiply_reduce_fusion.2
  211.0 0.4 fusion.88
  211.5 1.6 convolution_add_fusion.2
  213.1 1.4 multiply_reduce_fusion.2
  214.5 0.4 fusion.88
  215.0 1.6 convolution_add_fusion.2
  216.6 1.4 multiply_reduce_fusion.2
  218.0 0.4 fusion.88
  218.5 1.6 convolution_add_fusion.2
  220.1 1.4 multiply_reduce_fusion.2
  221.5 0.4 fusion.88
  222.0 1.6 convolution_add_fusion.2
  223.6 1.4 multiply_reduce_fusion.2
  225.5 1.6 convolution_add_fusion.2
  227.1 1.4 multiply_reduce_fusion.2
  229.0 1.6 convolution_add_fusion.2
  230.6 1.4 multiply_reduce_fusion.2
  232.5 1.6 convolution_add_fusion.2
  234.1 1.4 multiply_reduce_fusion.2
  236.0 1.6 convolution_add_fusion.2
  237.5 1.4 multiply_reduce_fusion.2
  239.4 1.6 convolution_add_fusion.2
  241.0 1.4 multiply_reduce_fusion.2
  242.9 1.6 convolution_add_fusion.2
  244.5 1.4 multiply_reduce_fusion.2
  246.4 1.6 convolution_add_fusion.2
  248.0 0.9 divide_convert_fusion
  248.9 8.0 %all-to-all-start = ((bf16[16,48,128]{2,1,0:T(8,128)(2,1)}), bf16[16,48,128]{2,1,0:T(8,128)(2,1)S(1)}, u32[]{:S(2)}, u32[]{:S(2)}) async-start(bf16[16,48,128]{2,1,0:T(8,128)(2,1)} %bitcast.6), calls=%async_computation | async-start | bytes 393216 | tf_op jit(solution)/shard_map/all_to_all | solution.py:112
  257.3 1.0 fusion.54
  258.3 8.8 %all-to-all-done = bf16[16,48,128]{2,1,0:T(8,128)(2,1)S(1)} async-done(((bf16[16,48,128]{2,1,0:T(8,128)(2,1)}), bf16[16,48,128]{2,1,0:T(8,128)(2,1)S(1)}, u32[]{:S(2)}, u32[]{:S(2)}) %all-to-all-start) | async-done | bytes 196640 | tf_op jit(solution)/shard_map/all_to_all | solution.py:112
  267.0 4.9 %all-to-all-start.2 = ((bf16[1,16,8,2048]{3,2,0,1:T(8,128)(2,1)}), bf16[1,16,8,2048]{3,2,0,1:T(8,128)(2,1)S(1)}, u32[]{:S(2)}, u32[]{:S(2)}) async-start(bf16[1,16,8,2048]{3,2,0,1:T(8,128)(2,1)} %bitcast.118), calls=%async_computation.4 | async-start | bytes 1048576 | tf_op jit(solution)/shard_map/all_to_all | solution.py:167
  272.0 5.7 %convolution_convert_fusion.3 = bf16[48,2048]{1,0:T(8,128)(2,1)} fusion(bf16[2048,2048]{1,0:T(8,128)(2,1)} %all-gather.6.cloned.1.call-done, bf16[16,48,128]{2,1,0:T(8,128)(2,1)S(1)} %all-to-all-done), kind=kOutput, calls=%fused_computation.26 | convolution fusion | flops 402751488 | bytes 8781824 | tf_op jit(solution)/shard_map/dot_general | solution.py:113
  277.7 5.5 %all-to-all-done.2 = bf16[1,16,8,2048]{3,2,0,1:T(8,128)(2,1)S(1)} async-done(((bf16[1,16,8,2048]{3,2,0,1:T(8,128)(2,1)}), bf16[1,16,8,2048]{3,2,0,1:T(8,128)(2,1)S(1)}, u32[]{:S(2)}, u32[]{:S(2)}) %all-to-all-start.2) | async-done | bytes 524320 | tf_op jit(solution)/shard_map/all_to_all | solution.py:167
  283.2 1.0 convolution_convert_fusion.2
  (117 shorter events, 7.0 us)
Async XLA Ops:
  8.0 88.5 %copy-start = (bf16[1,256,2048]{2,1,0:T(8,128)(2,1)S(1)}, bf16[1,256,2048]{2,1,0:T(8,128)(2,1)}, u32[]{:S(2)}) copy-start(bf16[1,256,2048]{2,1,0:T(8,128)(2,1)} %param.27) | copy-start | bytes 3145732
  8.0 81.4 %copy-start.7 = (bf16[1,2048,256]{2,1,0:T(8,128)(2,1)S(1)}, bf16[1,2048,256]{2,1,0:T(8,128)(2,1)}, u32[]{:S(2)}) copy-start(bf16[1,2048,256]{2,1,0:T(8,128)(2,1)} %param.25) | copy-start | bytes 3145732
  8.0 81.4 %all-gather.8.cloned.1.call-start = ((), (), s32[]{:S(2)}) async-start(), calls=%async_computation.7 | async-start | bytes 8912896 | tf_op jit(solution)/shard_map/all_gather | solution.py:154
  11.9 84.6 %copy-start.3 = (pred[16,96,128]{2,1,0:T(32,128)(4,1)}, pred[16,96,128]{2,1,0:T(32,128)(4,1)S(1)}, u32[]{:S(2)}) copy-start(pred[16,96,128]{2,1,0:T(32,128)(4,1)S(1)} %iota_compare_fusion) | copy-start | bytes 589828
  32.5 64.0 %copy-start.8 = (bf16[1,2048,256]{2,1,0:T(8,128)(2,1)S(1)}, bf16[1,2048,256]{2,1,0:T(8,128)(2,1)}, u32[]{:S(2)}) copy-start(bf16[1,2048,256]{2,1,0:T(8,128)(2,1)} %param.26) | copy-start | bytes 3145732
  32.6 106.2 %reduce-scatter.3.cloned.1.call-start = ((), (), s32[]{:S(2)}) async-start(), calls=%async_computation.8 | async-start | bytes 12582912 | tf_op jit(solution)/shard_map/reduce_scatter | solution.py:35
  118.0 1.3 copy-start.2
  118.0 1.9 copy-start.5
  118.1 2.0 copy-start.6
  118.1 67.8 %all-gather.4.cloned.1.call-start = ((), (), s32[]{:S(2)}) async-start(), calls=%async_computation.5 | async-start | bytes 6684672 | tf_op jit(solution)/shard_map/all_gather | solution.py:27
  121.8 17.8 %copy-start.4 = (f32[768,2]{0,1:T(2,128)S(1)}, f32[768,2]{0,1:T(2,128)}, u32[]{:S(2)}) copy-start(f32[768,2]{0,1:T(2,128)} %param.24) | copy-start | bytes 18436
  121.8 145.2 %reduce-scatter.5.cloned.1.call-start = ((), (), s32[]{:S(2)}) async-start(), calls=%async_computation.9 | async-start | bytes 4718592 | tf_op jit(solution)/shard_map/reduce_scatter | solution.py:35
  138.8 133.2 %all-gather.6.cloned.1.call-start = ((), (), s32[]{:S(2)}) async-start(), calls=%async_computation.6 | async-start | bytes 8912896 | tf_op jit(solution)/shard_map/all_gather | solution.py:115
  248.9 18.2 %all-to-all-start = ((bf16[16,48,128]{2,1,0:T(8,128)(2,1)}), bf16[16,48,128]{2,1,0:T(8,128)(2,1)S(1)}, u32[]{:S(2)}, u32[]{:S(2)}) async-start(bf16[16,48,128]{2,1,0:T(8,128)(2,1)} %bitcast.6), calls=%async_computation | async-start | bytes 393216 | tf_op jit(solution)/shard_map/all_to_all | solution.py:112
  267.0 16.2 %all-to-all-start.2 = ((bf16[1,16,8,2048]{3,2,0,1:T(8,128)(2,1)}), bf16[1,16,8,2048]{3,2,0,1:T(8,128)(2,1)S(1)}, u32[]{:S(2)}, u32[]{:S(2)}) async-start(bf16[1,16,8,2048]{3,2,0,1:T(8,128)(2,1)} %bitcast.118), calls=%async_computation.4 | async-start | bytes 1048576 | tf_op jit(solution)/shard_map/all_to_all | solution.py:167
  272.0 12.3 %copy-start.1 = (bf16[1,256,2048]{2,1,0:T(8,128)(2,1)S(1)}, bf16[1,256,2048]{2,1,0:T(8,128)(2,1)}, u32[]{:S(2)}) copy-start(bf16[1,256,2048]{2,1,0:T(8,128)(2,1)} %param.27) | copy-start | bytes 3145732
Sparse Core Ops, SparseCore 0:
  32.7 56.7 all-gather.7
  118.2 20.5 reduce-scatter.2
  141.3 55.9 reduce-scatter.4
Sparse Core Ops, SparseCore 1:
  121.9 63.9 all-gather.3
  187.6 56.2 all-gather.5
where the time goes:
time: 293 us; the launch traced here: 291 us
  waiting for transfers between devices  135 us (46%)
  matrix products  77.6 us (26%)
  local copies, waits for them, and re-layouts  18 us (6%)
  blocking collectives  17.9 us (6%)
  between operations  15.5 us (5%)
  other arithmetic  13.6 us (5%)
  starting transfers between devices  13.3 us (5%)
    all_gather x1, waiting for transfers between devices, expert_half(): slab_rows = lax.all_gather(arrived, TP, axis=0, tiled=True)  56.8 us
    all_gather x1, waiting for transfers between devices, side_by_side(): lax.all_gather(both, axis, axis=dim, tiled=True)  46.2 us
    dot_general x16, matrix products, one_block(): jnp.dot(weights.astype(jnp.bfloat16), value_blk, preferred_element_type=j...  24.9 us
    dot_general x16, matrix products, one_block(): jnp.einsum('qd,sd->qs', query_n, key_blk, preferred_element_type=jnp.floa...  23 us
    all_to_all x1, blocking collectives, expert_half(): lax.all_to_all(outgoing, 'ep', split_axis=0, concat_axis=1, tiled=True)  17.9 us
    reduce_scatter x2, waiting for transfers between devices, sum_in_order(): blocks = lax.psum_scatter(blocks, axes[k], scatter_dimension=0, tiled=True)  16.9 us
    dot_general x1, matrix products, expert_half(): jnp.einsum('blmf,lfd->blmd', hidden, down_weight, preferred_element_type=...  13.2 us
    all_to_all x1, waiting for transfers between devices, token_mixer(): lax.all_to_all(attended, TP, split_axis=0, concat_axis=1, tiled=True)  8.78 us
  transfers between devices with their start and end apart: 7, of which 5 were waited for; matrix products, arithmetic and copies ran while one was open for 25% of the time, Pallas kernels for 0%

commit v1 on v0

--- a/solution.py
+++ b/solution.py
@@ -151,7 +151,8 @@
     outgoing = outgoing.astype(jnp.bfloat16).reshape(EXPERTS, CAP, D)
     arrived = lax.all_to_all(outgoing, "ep", split_axis=0, concat_axis=1, tiled=True)
     arrived = arrived.reshape(1, local_experts, n_ep * CAP, D)
-    slab_rows = lax.all_gather(arrived, TP, axis=0, tiled=True)
+    repeated = jnp.stack([arrived] * lax.axis_size(TP))
+    slab_rows = jnp.concatenate(lax.all_to_all(repeated, TP, 0, 0), axis=0)
     gate_act = jnp.einsum(
         "blmd,ldf->blmf", slab_rows, gate_weight, preferred_element_type=jnp.float32
     )

time: 293 us -> 428 us (1.46)
  blocking collectives: 17.9 us -> 214 us
  waiting for transfers between devices: 135 us -> 72.8 us
    all_to_all x0 -> x1, blocking collectives: none -> 196 us  [expert_half(): slab_rows = jnp.concatenate(lax.all_to_all(repeated, TP, 0, 0), axis=0)]
    all_gather x1 -> x0, waiting for transfers between devices: 56.8 us -> none  [expert_half(): slab_rows = lax.all_gather(arrived, TP, axis=0, tiled=True)]
    reduce_scatter x2, waiting for transfers between devices: 16.9 us -> 11.6 us  [sum_in_order(): blocks = lax.psum_scatter(blocks, axes[k], scatter_dimension=0, tiled=True)]
  transfers between devices with their start and end apart: 7 -> 6, of which waited for: 5 -> 4; matrix products, arithmetic and copies ran while one was open for 25% -> 17% of each run, Pallas kernels for 0% -> 0%
where the time goes in v1:
time: 428 us; the launch traced here: 427 us
  blocking collectives  214 us (50%)
  matrix products  74.2 us (17%)
  waiting for transfers between devices  72.8 us (17%)
  local copies, waits for them, and re-layouts  22.2 us (5%)
  between operations  15.8 us (4%)
  other arithmetic  13.5 us (3%)
  starting transfers between devices  13.2 us (3%)
    all_to_all x1, blocking collectives, expert_half(): slab_rows = jnp.concatenate(lax.all_to_all(repeated, TP, 0, 0), axis=0)  196 us
    all_gather x1, waiting for transfers between devices, side_by_side(): lax.all_gather(both, axis, axis=dim, tiled=True)  46.4 us
    dot_general x16, matrix products, one_block(): jnp.dot(weights.astype(jnp.bfloat16), value_blk, preferred_element_type=j...  24.9 us
    dot_general x16, matrix products, one_block(): jnp.einsum('qd,sd->qs', query_n, key_blk, preferred_element_type=jnp.floa...  23 us
    all_to_all x1, blocking collectives, expert_half(): lax.all_to_all(outgoing, 'ep', split_axis=0, concat_axis=1, tiled=True)  17.8 us
    dot_general x1, matrix products, expert_half(): jnp.einsum('blmf,lfd->blmd', hidden, down_weight, preferred_element_type=...  13.2 us
    reduce_scatter x2, waiting for transfers between devices, sum_in_order(): blocks = lax.psum_scatter(blocks, axes[k], scatter_dimension=0, tiled=True)  11.6 us
    all_to_all x1, waiting for transfers between devices, token_mixer(): lax.all_to_all(attended, TP, split_axis=0, concat_axis=1, tiled=True)  8.78 us
  transfers between devices with their start and end apart: 6, of which 4 were waited for; matrix products, arithmetic and copies ran while one was open for 17% of the time, Pallas kernels for 0%

profile of v1, /device:TPU:1, one launch (start us, length us, event | category | flops | bytes accessed | tf_op | source)
XLA Modules:
  0.0 426.6 jit_solution(6846863440759393902)
XLA Ops:
  8.1 0.9 copy.49
  9.3 2.1 select_reduce_fusion
  11.8 1.1 fusion.42
  13.3 1.3 fusion.16
  14.6 17.8 %all_to_all.42 = bf16[16,8,2048]{2,1,0:T(8,128)(2,1)S(1)} all-to-all(bf16[16,8,2048]{2,1,0:T(8,128)(2,1)S(1)} %fusion.16), channel_id=1, replica_groups=mesh['ep'=16,'tp_0'=8,'tp_1'=2] {'ep'}, dimensions={0} | all-to-all | bytes 1048576 | tf_op jit(solution)/shard_map/all_to_all | solution.py:152
  32.4 1.1 stack.32
  33.4 196.2 %all_to_all.43 = bf16[16,1,1,128,2048]{4,3,2,1,0:T(8,128)(2,1)S(1)} all-to-all(bf16[16,1,1,128,2048]{4,3,2,1,0:T(8,128)(2,1)S(1)} %stack.32), channel_id=1, replica_groups=mesh['ep'=16,'tp_0'=8,'tp_1'=2] {'tp_0','tp_1'}, dimensions={0} | all-to-all | bytes 16777216 | tf_op jit(solution)/shard_map/all_to_all | solution.py:155
  229.6 3.2 copy-done.2
  232.9 3.8 fusion.14
  236.6 13.2 %convolution_convert_fusion = bf16[16,128,2048]{2,1,0:T(8,128)(2,1)} fusion(bf16[16,1,1,128,2048]{4,3,2,1,0:T(8,128)(2,1)} %copy-done.2, f32[16,128,256]{2,1,0:T(8,128)} %fusion.14, bf16[1,256,2048]{2,1,0:T(8,128)(2,1)S(1)} %copy-done, bf16[1,2048,256]{2,1,0:T(8,128)(2,1)S(1)} %copy-done.9), kind=kOutput, calls=%fused_computation.22 | convolution fusion | flops 4302307328 | bytes 20971520 | tf_op jit(solution)/shard_map/blmf,lfd->blmd/dot_general | solution.py:161
  249.8 8.3 %copy.53 = bf16[8,2,128,2048]{3,2,0,1:T(8,128)(2,1)} copy(bf16[8,2,128,2048]{3,2,1,0:T(8,128)(2,1)} %bitcast.112) | data formatting | bytes 16777216 | tf_op jit(solution)/shard_map/convert_element_type | solution.py:164
  258.4 1.1 constant_dynamic-slice_fusion.1
  260.4 0.8 subtract_convert_fusion
  261.2 0.8 pad_maximum_fusion
  262.0 11.6 %reduce-scatter.3.cloned.1.call-done = bf16[8,128,2048]{2,1,0:T(8,128)(2,1)} async-done(((bf16[16,128,2048]{2,1,0:T(8,128)(2,1)}), bf16[8,128,2048]{2,1,0:T(8,128)(2,1)}) %reduce-scatter.3.cloned.1.call-update) | async-done | bytes 4194320 | tf_op jit(solution)/shard_map/reduce_scatter | solution.py:35
  273.7 0.5 all-gather.5.cloned.1.call-update
  274.5 46.4 %all-gather.3.cloned.1.call-done = bf16[12288,256]{0,1:T(8,128)(2,1)} async-done(((bf16[768,256]{0,1:T(8,128)(2,1)}), bf16[12288,256]{0,1:T(8,128)(2,1)}) %all-gather.3.cloned.1.call-update) | async-done | bytes 6291472 | tf_op jit(solution)/shard_map/all_gather | solution.py:27
  320.8 6.2 %fusion.74 = (bf16[12288,128]{0,1:T(8,128)(2,1)}, bf16[12288,128]{0,1:T(8,128)(2,1)}) fusion(bf16[12288,256]{0,1:T(8,128)(2,1)} %all-gather.3.cloned.1.call-done), kind=kLoop, calls=%fused_computation.121 | loop fusion | bytes 12582912 | tf_op jit(solution)/shard_map/split | solution.py:27
  327.0 55.9 %while.18 = (s32[]{:T(128)}, f32[768]{0:T(1024)S(1)}, f32[768]{0:T(1024)S(1)}, f32[768,128]{1,0:T(8,128)S(1)}, bf16[12288,128]{0,1:T(8,128)(2,1)}, /*index=5*/bf...) while((s32[]{:T(128)}, f32[768]{0:T(1024)S(1)}, ...), condition=%wide.region_5.6_spmd.clone, body=%wide.region_2.5_spmd.clone.sunk | while | flops 307007232 | bytes 8503471 | solution.py:110
  327.0 1.4 multiply_reduce_fusion.2
  328.5 0.4 fusion.88
  328.9 1.6 convolution_add_fusion.2
  330.5 1.4 multiply_reduce_fusion.2
  332.4 1.6 convolution_add_fusion.2
  334.0 1.4 multiply_reduce_fusion.2
  335.5 0.4 fusion.88
  335.9 1.6 convolution_add_fusion.2
  337.5 1.4 multiply_reduce_fusion.2
  339.0 0.4 fusion.88
  339.4 1.6 convolution_add_fusion.2
  341.0 1.4 multiply_reduce_fusion.2
  342.5 0.4 fusion.88
  342.9 1.6 convolution_add_fusion.2
  344.5 1.4 multiply_reduce_fusion.2
  346.0 0.4 fusion.88
  346.4 1.6 convolution_add_fusion.2
  348.0 1.4 multiply_reduce_fusion.2
  349.9 1.6 convolution_add_fusion.2
  351.5 1.4 multiply_reduce_fusion.2
  353.4 1.6 convolution_add_fusion.2
  355.0 1.4 multiply_reduce_fusion.2
  356.9 1.6 convolution_add_fusion.2
  358.5 1.4 multiply_reduce_fusion.2
  360.4 1.6 convolution_add_fusion.2
  362.0 1.4 multiply_reduce_fusion.2
  363.9 1.6 convolution_add_fusion.2
  365.5 1.4 multiply_reduce_fusion.2
  367.4 1.6 convolution_add_fusion.2
  369.0 1.4 multiply_reduce_fusion.2
  370.9 1.6 convolution_add_fusion.2
  372.5 1.4 multiply_reduce_fusion.2
  374.4 1.6 convolution_add_fusion.2
  376.0 1.4 multiply_reduce_fusion.2
  377.9 1.6 convolution_add_fusion.2
  379.5 1.4 multiply_reduce_fusion.2
  381.4 1.6 convolution_add_fusion.2
  382.9 0.9 divide_convert_fusion
  383.8 8.0 %all-to-all-start = ((bf16[16,48,128]{2,1,0:T(8,128)(2,1)}), bf16[16,48,128]{2,1,0:T(8,128)(2,1)S(1)}, u32[]{:S(2)}, u32[]{:S(2)}) async-start(bf16[16,48,128]{2,1,0:T(8,128)(2,1)} %bitcast.6), calls=%async_computation | async-start | bytes 393216 | tf_op jit(solution)/shard_map/all_to_all | solution.py:112
  392.2 1.0 fusion.54
  393.2 8.8 %all-to-all-done = bf16[16,48,128]{2,1,0:T(8,128)(2,1)S(1)} async-done(((bf16[16,48,128]{2,1,0:T(8,128)(2,1)}), bf16[16,48,128]{2,1,0:T(8,128)(2,1)S(1)}, u32[]{:S(2)}, u32[]{:S(2)}) %all-to-all-start) | async-done | bytes 196640 | tf_op jit(solution)/shard_map/all_to_all | solution.py:112
  402.0 4.9 %all-to-all-start.3 = ((bf16[1,16,8,2048]{3,2,0,1:T(8,128)(2,1)}), bf16[1,16,8,2048]{3,2,0,1:T(8,128)(2,1)S(1)}, u32[]{:S(2)}, u32[]{:S(2)}) async-start(bf16[1,16,8,2048]{3,2,0,1:T(8,128)(2,1)} %bitcast.118), calls=%async_computation.5 | async-start | bytes 1048576 | tf_op jit(solution)/shard_map/all_to_all | solution.py:168
  407.0 5.7 %convolution_convert_fusion.3 = bf16[48,2048]{1,0:T(8,128)(2,1)} fusion(bf16[2048,2048]{1,0:T(8,128)(2,1)} %all-gather.5.cloned.1.call-done, bf16[16,48,128]{2,1,0:T(8,128)(2,1)S(1)} %all-to-all-done), kind=kOutput, calls=%fused_computation.26 | convolution fusion | flops 402751488 | bytes 8781824 | tf_op jit(solution)/shard_map/dot_general | solution.py:113
  412.7 5.5 %all-to-all-done.3 = bf16[1,16,8,2048]{3,2,0,1:T(8,128)(2,1)S(1)} async-done(((bf16[1,16,8,2048]{3,2,0,1:T(8,128)(2,1)}), bf16[1,16,8,2048]{3,2,0,1:T(8,128)(2,1)S(1)}, u32[]{:S(2)}, u32[]{:S(2)}) %all-to-all-start.3) | async-done | bytes 524320 | tf_op jit(solution)/shard_map/all_to_all | solution.py:168
  418.2 1.0 convolution_convert_fusion.2
  (118 shorter events, 7.9 us)
Async XLA Ops:
  8.0 228.6 %copy-start = (bf16[1,256,2048]{2,1,0:T(8,128)(2,1)S(1)}, bf16[1,256,2048]{2,1,0:T(8,128)(2,1)}, u32[]{:S(2)}) copy-start(bf16[1,256,2048]{2,1,0:T(8,128)(2,1)} %param.27) | copy-start | bytes 3145732
  8.0 265.6 %reduce-scatter.3.cloned.1.call-start = ((), (), s32[]{:S(2)}) async-start(), calls=%async_computation.8 | async-start | bytes 12582912 | tf_op jit(solution)/shard_map/reduce_scatter | solution.py:35
  11.8 21.6 %copy-start.4 = (pred[16,96,128]{2,1,0:T(32,128)(4,1)}, pred[16,96,128]{2,1,0:T(32,128)(4,1)S(1)}, u32[]{:S(2)}) copy-start(pred[16,96,128]{2,1,0:T(32,128)(4,1)S(1)} %iota_compare_fusion) | copy-start | bytes 589828
  33.4 199.4 %copy-start.8 = (bf16[1,2048,256]{2,1,0:T(8,128)(2,1)S(1)}, bf16[1,2048,256]{2,1,0:T(8,128)(2,1)}, u32[]{:S(2)}) copy-start(bf16[1,2048,256]{2,1,0:T(8,128)(2,1)} %param.25) | copy-start | bytes 3145732
  229.6 3.2 copy-start.2
  232.9 3.8 copy-start.9
  258.1 1.5 copy-start.3
  258.1 2.1 copy-start.6
  258.1 2.2 copy-start.7
  258.1 62.7 %all-gather.3.cloned.1.call-start = ((), (), s32[]{:S(2)}) async-start(), calls=%async_computation.6 | async-start | bytes 6684672 | tf_op jit(solution)/shard_map/all_gather | solution.py:27
  262.0 12.5 %copy-start.5 = (f32[768,2]{0,1:T(2,128)S(1)}, f32[768,2]{0,1:T(2,128)}, u32[]{:S(2)}) copy-start(f32[768,2]{0,1:T(2,128)} %param.24) | copy-start | bytes 18436
  262.0 140.0 %reduce-scatter.5.cloned.1.call-start = ((), (), s32[]{:S(2)}) async-start(), calls=%async_computation.9 | async-start | bytes 4718592 | tf_op jit(solution)/shard_map/reduce_scatter | solution.py:35
  273.6 133.3 %all-gather.5.cloned.1.call-start = ((), (), s32[]{:S(2)}) async-start(), calls=%async_computation.7 | async-start | bytes 8912896 | tf_op jit(solution)/shard_map/all_gather | solution.py:115
  383.8 18.2 %all-to-all-start = ((bf16[16,48,128]{2,1,0:T(8,128)(2,1)}), bf16[16,48,128]{2,1,0:T(8,128)(2,1)S(1)}, u32[]{:S(2)}, u32[]{:S(2)}) async-start(bf16[16,48,128]{2,1,0:T(8,128)(2,1)} %bitcast.6), calls=%async_computation | async-start | bytes 393216 | tf_op jit(solution)/shard_map/all_to_all | solution.py:112
  402.0 16.2 %all-to-all-start.3 = ((bf16[1,16,8,2048]{3,2,0,1:T(8,128)(2,1)}), bf16[1,16,8,2048]{3,2,0,1:T(8,128)(2,1)S(1)}, u32[]{:S(2)}, u32[]{:S(2)}) async-start(bf16[1,16,8,2048]{3,2,0,1:T(8,128)(2,1)} %bitcast.118), calls=%async_computation.5 | async-start | bytes 1048576 | tf_op jit(solution)/shard_map/all_to_all | solution.py:168
  406.9 12.3 %copy-start.1 = (bf16[1,256,2048]{2,1,0:T(8,128)(2,1)S(1)}, bf16[1,256,2048]{2,1,0:T(8,128)(2,1)}, u32[]{:S(2)}) copy-start(bf16[1,256,2048]{2,1,0:T(8,128)(2,1)} %param.27) | copy-start | bytes 3145732
Sparse Core Ops, SparseCore 0:
  258.2 15.3 reduce-scatter.2
  276.1 55.9 reduce-scatter.4
Sparse Core Ops, SparseCore 1:
  262.1 58.7 all-gather.2
  322.5 56.2 all-gather.4
